TPU v7x, 32 devices: a whole 2x2x4 slice. The times are simulated.
32 devices in a mesh: sp: 8 (over z, x), tp: 4 (over y, core).
Axes of the slice: x: 2, y: 2, z: 4, core: 2. Of those that a mesh axis runs over, the one named last changes fastest.
Arguments:
- latent: bfloat16 [6144, 2048], P(('sp', 'tp')), may hold values from -6 to 6
- context: bfloat16 [1024, 2048], P('sp'), may hold values from -6 to 6
- conditioning: float32 [2, 2048], replicated, may hold values from -6 to 6
- norm_gain: float32 [2048], replicated, may hold values from 0.1 to 1.9
- mod_shift: bfloat16 [2048, 2048], P('sp', 'tp'), may hold values from -0.1875 to 0.1875
- mod_scale: bfloat16 [2048, 2048], P('sp', 'tp'), may hold values from -0.1875 to 0.1875
- mod_gate: bfloat16 [2048, 2048], P('sp', 'tp'), may hold values from -0.1875 to 0.1875
- w_query: bfloat16 [2048, 2048], P(None, 'tp'), may hold values from -4 to 4
- w_key: bfloat16 [2048, 2048], P(None, 'tp'), may hold values from -0.125 to 0.125
- w_value: bfloat16 [2048, 2048], P(None, 'tp'), may hold values from -0.125 to 0.125
- w_out: bfloat16 [2048, 2048], P('tp'), may hold values from -0.125 to 0.125
- lambdas: float32 [16], P('tp'), may hold values from 0.3 to 0.8
- context_bias: float32 [16], P('tp'), may hold values from 0.8 to 2.2
- head_gain: float32 [128], replicated, may hold values from 0.1 to 1.9
Outputs:
- updated: bfloat16 [6144, 2048], P(('sp', 'tp'))
All inputs are finite; a program needn't handle non-finite values.
Results may differ from a plain program's by a relative error of at most 0.01.
The roundings to bfloat16 on the way count: a program that leaves them out, or rounds other values in their place, can miss the bound.
Values may be sent and summed in bfloat16 or wider, within the bound.
A program may use at most 128 MiB of HBM per device.

v0:
```python
import jax
import jax.numpy as jnp
from jax import lax
from jax.sharding import PartitionSpec as P

EPS = 1e-06
NEGATIVE = -1e30


def modulated(inputs, norm_scale, offset_vec, scale_vec):
    rows_float = inputs.astype(jnp.float32)
    normal = rows_float * lax.rsqrt(jnp.mean(rows_float * rows_float, axis=-1, keepdims=True) + EPS)
    return (normal * norm_scale * (1.0 + scale_vec) + offset_vec).astype(jnp.bfloat16)


def block_size(length):
    for candidate in range(min(length, 1024), 0, -1):
        if length % candidate == 0:
            return candidate
    return length


def absorb(running, portion, context_flags, queries, bias_heads):
    head_count = queries.shape[1]
    head_dim = queries.shape[3]
    row_count = portion.shape[0]
    head_cols = head_count * 2 * head_dim
    key_rows = portion[:, :head_cols].reshape(row_count, head_count, 2, head_dim)
    value_rows = portion[:, head_cols:].reshape(row_count, head_count, 2 * head_dim)
    shifts = bias_heads[:, None, None] * context_flags[None, None, :]
    updated = []
    for which_map in range(2):
        previous, weight, accumulated = running[3 * which_map : 3 * which_map + 3]
        scores = (
            jnp.einsum(
                "qhd,khd->hqk",
                queries[:, :, which_map],
                key_rows[:, :, which_map],
                preferred_element_type=jnp.float32,
            )
            * head_dim ** (-0.5)
            + shifts
        )
        peak_new = jnp.maximum(previous, jnp.max(scores, axis=2))
        faded = jnp.exp(previous - peak_new)
        raised = jnp.exp(scores - peak_new[:, :, None])
        weight = weight * faded + jnp.sum(raised, axis=2)
        accumulated = accumulated * faded.T[:, :, None] + jnp.einsum(
            "hqk,khd->qhd",
            raised.astype(jnp.bfloat16),
            value_rows,
            preferred_element_type=jnp.float32,
        )
        updated += [peak_new, weight, accumulated]
    return tuple(updated)


def absorb_rows(running, portion, context_flags, queries, bias_heads):
    row_count = portion.shape[0]
    block_len = block_size(row_count)
    if block_len == row_count:
        return absorb(running, portion, context_flags, queries, bias_heads)
    stacked = portion.reshape(row_count // block_len, block_len, portion.shape[1])
    flag_blocks = context_flags.reshape(row_count // block_len, block_len)

    def advance(state_now, operand):
        return (absorb(state_now, operand[0], operand[1], queries, bias_heads), None)

    running, unused = lax.scan(advance, running, (stacked, flag_blocks))
    return running


def per_device(
    latent,
    context,
    conditioning,
    norm_gain,
    mod_shift,
    mod_scale,
    mod_gate,
    w_query,
    w_key,
    w_value,
    w_out,
    lambdas,
    context_bias,
    head_gain,
):
    head_dim = head_gain.shape[0] // 2
    head_count = lambdas.shape[0]
    rows_sp = mod_shift.shape[0]
    cond_rows = lax.dynamic_slice_in_dim(conditioning, lax.axis_index("sp") * rows_sp, rows_sp, 1)
    activated = jax.nn.silu(cond_rows).astype(jnp.bfloat16)
    partials = jnp.stack(
        [
            jnp.dot(activated, matrix, preferred_element_type=jnp.float32)
            for matrix in (mod_shift, mod_scale, mod_gate)
        ],
        axis=1,
    )
    summed = lax.psum(partials, "sp")
    modulation = lax.all_gather(summed, "tp", axis=2, tiled=True)
    own_rows = modulated(latent, norm_gain, modulation[0, 0], modulation[0, 1])
    context_rows = modulated(context, norm_gain, modulation[1, 0], modulation[1, 1])
    key_value = jnp.concatenate([w_key, w_value], axis=1)
    projector = jnp.concatenate([w_query, key_value], axis=1)
    projected = jnp.dot(
        lax.all_gather(own_rows, "tp", axis=0, tiled=True),
        projector,
        preferred_element_type=jnp.float32,
    ).astype(jnp.bfloat16)
    head_cols = w_query.shape[1]
    token_count = projected.shape[0]
    queries = projected[:, :head_cols].reshape(token_count, head_count, 2, head_dim)
    latent_kv = projected[:, head_cols:]
    context_kv = jnp.dot(context_rows, key_value, preferred_element_type=jnp.float32).astype(
        jnp.bfloat16
    )
    first_map = (
        jnp.full((head_count, token_count), NEGATIVE, jnp.float32),
        jnp.zeros((head_count, token_count), jnp.float32),
        jnp.zeros((token_count, head_count, 2 * head_dim), jnp.float32),
    )
    initial = first_map + first_map
    every_context = lax.all_gather(context_kv, "sp", axis=0, tiled=True)
    running = absorb_rows(
        initial,
        every_context,
        jnp.ones((every_context.shape[0],), jnp.float32),
        queries,
        context_bias,
    )
    portion = lax.all_gather(latent_kv, "sp", axis=0, tiled=True)
    running = absorb_rows(
        running, portion, jnp.zeros((portion.shape[0],), jnp.float32), queries, context_bias
    )
    peak_one, total_one, accum_one, peak_two, total_two, accum_two = running
    mixed = accum_one / total_one.T[:, :, None] - lambdas[None, :, None] * (
        accum_two / total_two.T[:, :, None]
    )
    normed = mixed * lax.rsqrt(jnp.mean(mixed * mixed, axis=-1, keepdims=True) + EPS) * head_gain
    flattened = normed.reshape(token_count, head_cols).astype(jnp.bfloat16)
    attended = lax.psum_scatter(
        jnp.dot(flattened, w_out, preferred_element_type=jnp.float32).astype(jnp.bfloat16),
        "tp",
        scatter_dimension=0,
        tiled=True,
    )
    return (latent.astype(jnp.float32) + modulation[0, 2] * attended.astype(jnp.float32)).astype(
        jnp.bfloat16
    )


def solution(mesh):
    return jax.shard_map(
        per_device,
        mesh=mesh,
        in_specs=(
            P(("sp", "tp"), None),
            P("sp", None),
            P(),
            P(),
            P("sp", "tp"),
            P("sp", "tp"),
            P("sp", "tp"),
            P(None, "tp"),
            P(None, "tp"),
            P(None, "tp"),
            P("tp", None),
            P("tp"),
            P("tp"),
            P(),
        ),
        out_specs=P(("sp", "tp"), None),
        check_vma=False,
    )
```

profile of v0, /device:TPU:0, one launch (start us, length us, event | category | flops | bytes accessed | tf_op | source)
XLA Modules:
  0.0 557.7 jit_solution(13907041467783386179)
XLA Ops:
  10.0 38.8 %psum.7 = f32[2,3,512]{2,0,1:T(2,128)S(1)} all-reduce(f32[2,3,512]{2,0,1:T(2,128)S(1)} %pad_maximum_fusion), channel_id=1, replica_groups=mesh['sp'=8,'tp'=4] {'sp'}, use_global_device_ids=true, to_apply=%region_0.1 | all-reduce | flops 3072 | bytes 24576 | tf_op jit(solution)/shard_map/psum | solution.py:101
  48.9 5.2 all_gather.12
  63.9 20.6 %all-gather.4.cloned.1.call-done = bf16[768,2048]{1,0:T(8,128)(2,1)} async-done(((bf16[192,2048]{1,0:T(8,128)(2,1)}), bf16[768,2048]{1,0:T(8,128)(2,1)}) %all-gather.4.cloned.1.call-update) | async-done | bytes 3145744 | tf_op jit(solution)/shard_map/all_gather | solution.py:108
  84.5 8.8 %fusion.44 = bf16[768,1536]{1,0:T(8,128)(2,1)S(1)} fusion(bf16[768,2048]{1,0:T(8,128)(2,1)} %all-gather.4.cloned.1.call-done, bf16[2048,512]{1,0:T(8,128)(2,1)} %param.25, bf16[2048,512]{1,0:T(8,128)(2,1)} %param.24, bf16[2048,512]{1,0:T(8,128)(2,1)} %param.23), kind=kOutput, calls=%fused_computation.56 | convolution fusion | flops 4851892224 | bytes 11796480 | tf_op jit(solution)/shard_map/dot_general | solution.py:107
  96.4 39.3 %all-gather.6.cloned.1.call-done = bf16[1024,1024]{1,0:T(8,128)(2,1)} async-done(((bf16[128,1024]{1,0:T(8,128)(2,1)}), bf16[1024,1024]{1,0:T(8,128)(2,1)}) %all-gather.6.cloned.1.call-update) | async-done | bytes 2097168 | tf_op jit(solution)/shard_map/all_gather | solution.py:125
  149.7 6.2 %fusion.25 = (f32[4,768]{1,0:T(4,128)S(1)}, f32[4,768]{1,0:T(4,128)S(1)}, f32[4,768,1024]{2,1,0:T(8,128)}) fusion(f32[4]{0:T(128)S(1)} %copy-done.9, f32[4,768,1024]{2,1,0:T(8,128)S(1)} %fusion.67, bf16[1024,4,2,64]{0,3,2,1:T(8,128)(2,1)S(1)} %bitcast.155, bf16[768,4,2,64]{0,3,2,1:T(8,128)(2,1)S(1)} %bitcast.153), kind=kOutput, calls=%fused_computation.39 | convolution fusion | flops 421521408 | bytes 26108416 | tf_op jit(solution)/shard_map/qhd,khd->hqk/dot_general | solution.py:35
  155.8 8.2 %fusion.29 = (f32[4,768]{1,0:T(4,128)S(1)}, f32[4,768]{1,0:T(4,128)S(1)}) fusion(f32[4,768,1024]{2,1,0:T(8,128)} %get-tuple-element.134, f32[4,768]{1,0:T(4,128)S(1)} %broadcast_maximum_fusion, f32[4]{0:T(128)S(1)} %copy-done.9, f32[4,768]{1,0:T(4,128)S(1)} %broadcast_maximum_fusion.1, f32[4,768,1024]{2,1,0:T(8,128)S(1)} %fusion.67), kind=kLoop, calls=%fused_computation.43 | loop fusion | flops 25159680 | bytes 25214992 | tf_op jit(solution)/shard_map/reduce_sum | solution.py:47
  164.0 8.6 %bitcast_add_fusion.2 = f32[768,4,128]{0,2,1:T(8,128)} fusion(bf16[1024,4,128]{0,2,1:T(8,128)(2,1)S(1)} %bitcast.156, f32[4,768,1024]{2,1,0:T(8,128)} %get-tuple-element.134, f32[4,768]{1,0:T(4,128)S(1)} %broadcast_maximum_fusion, f32[4]{0:T(128)S(1)} %copy-done.9, f32[768,4]{0,1:T(4,128)S(1)} %get-tuple-element.136), kind=kOutput, calls=%fused_computation.67 | convolution fusion | flops 818282496 | bytes 15228944 | tf_op jit(solution)/shard_map/hqk,khd->qhd/dot_general | solution.py:48
  176.8 135.7 %all-gather.8.cloned.1.call-done = bf16[6144,1024]{1,0:T(8,128)(2,1)} async-done(((bf16[768,1024]{1,0:T(8,128)(2,1)}), bf16[6144,1024]{1,0:T(8,128)(2,1)}) %all-gather.8.cloned.1.call-update) | async-done | bytes 12582928 | tf_op jit(solution)/shard_map/all_gather | solution.py:133
  312.6 193.9 %while.20 = (s32[]{:T(128)}, f32[4,768]{1,0:T(4,128)S(1)}, f32[4,768]{1,0:T(4,128)S(1)}, f32[768,4,128]{0,2,1:T(8,128)}, f32[4,768]{1,0:T(4,128)S(1)}, /*index=5...) while((s32[]{:T(128)}, f32[4,768]{1,0:T(4,128)S(1)}, ...), condition=%wide.region_12.13_spmd, body=%wide.region_7.12_spmd.sunk | while | flops 2486716416 | bytes 128058136 | solution.py:69
  325.1 5.5 bitcast_reduce_fusion.3
  330.7 5.8 %bitcast_add_fusion.7 = f32[768,4,128]{0,2,1:T(8,128)} fusion(f32[768,4,128]{0,2,1:T(8,128)} %get-tuple-element.241, bf16[1024,4,128]{0,2,1:T(8,128)(2,1)} %bitcast.148, f32[4,1024,768]{2,1,0:T(8,128)S(1)} %get-tuple-element.214, f32[4,768]{1,0:T(4,128)S(1)} %get-tuple-element.250, f32[4]{0:T(128)S(1)} %broadcast_multiply_fusion.2, ...), kind=kOutput, calls=%fused_computation.14.clone.1 | convolution fusion | flops 818675712 | bytes 16801808 | tf_op jit(solution)/shard_map/while/body/eval_jaxpr/hqk,khd->qhd/dot_general | solution.py:48
  339.7 5.1 fusion.118
  357.5 5.5 bitcast_reduce_fusion.3
  363.0 5.8 %bitcast_add_fusion.7 = f32[768,4,128]{0,2,1:T(8,128)} fusion(f32[768,4,128]{0,2,1:T(8,128)} %get-tuple-element.241, bf16[1024,4,128]{0,2,1:T(8,128)(2,1)} %bitcast.148, f32[4,1024,768]{2,1,0:T(8,128)S(1)} %get-tuple-element.214, f32[4,768]{1,0:T(4,128)S(1)} %get-tuple-element.250, f32[4]{0:T(128)S(1)} %broadcast_multiply_fusion.2, ...), kind=kOutput, calls=%fused_computation.14.clone.1 | convolution fusion | flops 818675712 | bytes 16801808 | tf_op jit(solution)/shard_map/while/body/eval_jaxpr/hqk,khd->qhd/dot_general | solution.py:48
  389.8 5.5 bitcast_reduce_fusion.3
  395.3 5.8 %bitcast_add_fusion.7 = f32[768,4,128]{0,2,1:T(8,128)} fusion(f32[768,4,128]{0,2,1:T(8,128)} %get-tuple-element.241, bf16[1024,4,128]{0,2,1:T(8,128)(2,1)} %bitcast.148, f32[4,1024,768]{2,1,0:T(8,128)S(1)} %get-tuple-element.214, f32[4,768]{1,0:T(4,128)S(1)} %get-tuple-element.250, f32[4]{0:T(128)S(1)} %broadcast_multiply_fusion.2, ...), kind=kOutput, calls=%fused_computation.14.clone.1 | convolution fusion | flops 818675712 | bytes 16801808 | tf_op jit(solution)/shard_map/while/body/eval_jaxpr/hqk,khd->qhd/dot_general | solution.py:48
  422.1 5.5 bitcast_reduce_fusion.3
  427.6 5.8 %bitcast_add_fusion.7 = f32[768,4,128]{0,2,1:T(8,128)} fusion(f32[768,4,128]{0,2,1:T(8,128)} %get-tuple-element.241, bf16[1024,4,128]{0,2,1:T(8,128)(2,1)} %bitcast.148, f32[4,1024,768]{2,1,0:T(8,128)S(1)} %get-tuple-element.214, f32[4,768]{1,0:T(4,128)S(1)} %get-tuple-element.250, f32[4]{0:T(128)S(1)} %broadcast_multiply_fusion.2, ...), kind=kOutput, calls=%fused_computation.14.clone.1 | convolution fusion | flops 818675712 | bytes 16801808 | tf_op jit(solution)/shard_map/while/body/eval_jaxpr/hqk,khd->qhd/dot_general | solution.py:48
  454.4 5.5 bitcast_reduce_fusion.3
  459.9 5.8 %bitcast_add_fusion.7 = f32[768,4,128]{0,2,1:T(8,128)} fusion(f32[768,4,128]{0,2,1:T(8,128)} %get-tuple-element.241, bf16[1024,4,128]{0,2,1:T(8,128)(2,1)} %bitcast.148, f32[4,1024,768]{2,1,0:T(8,128)S(1)} %get-tuple-element.214, f32[4,768]{1,0:T(4,128)S(1)} %get-tuple-element.250, f32[4]{0:T(128)S(1)} %broadcast_multiply_fusion.2, ...), kind=kOutput, calls=%fused_computation.14.clone.1 | convolution fusion | flops 818675712 | bytes 16801808 | tf_op jit(solution)/shard_map/while/body/eval_jaxpr/hqk,khd->qhd/dot_general | solution.py:48
  486.7 5.5 bitcast_reduce_fusion.3
  492.3 5.8 %bitcast_add_fusion.7 = f32[768,4,128]{0,2,1:T(8,128)} fusion(f32[768,4,128]{0,2,1:T(8,128)} %get-tuple-element.241, bf16[1024,4,128]{0,2,1:T(8,128)(2,1)} %bitcast.148, f32[4,1024,768]{2,1,0:T(8,128)S(1)} %get-tuple-element.214, f32[4,768]{1,0:T(4,128)S(1)} %get-tuple-element.250, f32[4]{0:T(128)S(1)} %broadcast_multiply_fusion.2, ...), kind=kOutput, calls=%fused_computation.14.clone.1 | convolution fusion | flops 818675712 | bytes 16801808 | tf_op jit(solution)/shard_map/while/body/eval_jaxpr/hqk,khd->qhd/dot_general | solution.py:48
  512.7 36.2 %reduce-scatter.2.cloned.1.call-done = bf16[192,2048]{1,0:T(8,128)(2,1)} async-done(((bf16[768,2048]{1,0:T(8,128)(2,1)}), bf16[192,2048]{1,0:T(8,128)(2,1)}) %reduce-scatter.2.cloned.1.call-update) | async-done | bytes 786448 | tf_op jit(solution)/shard_map/reduce_scatter | solution.py:143
  (161 shorter events, 163.5 us)
Async XLA Ops:
  6.5 502.6 %copy-start = (bf16[512,2048]{1,0:T(8,128)(2,1)S(1)}, bf16[512,2048]{1,0:T(8,128)(2,1)}, u32[]{:S(2)}) copy-start(bf16[512,2048]{1,0:T(8,128)(2,1)} %param.26) | copy-start | bytes 6291460
  6.5 77.9 %all-gather.4.cloned.1.call-start = ((), (), s32[]{:S(2)}) async-start(), calls=%async_computation.1 | async-start | bytes 3932160 | tf_op jit(solution)/shard_map/all_gather | solution.py:108
  58.5 77.2 %all-gather.6.cloned.1.call-start = ((), (), s32[]{:S(2)}) async-start(), calls=%async_computation.2 | async-start | bytes 2359296 | tf_op jit(solution)/shard_map/all_gather | solution.py:125
  63.8 248.7 %all-gather.8.cloned.1.call-start = ((), (), s32[]{:S(2)}) async-start(), calls=%async_computation.3 | async-start | bytes 14155776 | tf_op jit(solution)/shard_map/all_gather | solution.py:133
  96.2 452.7 %reduce-scatter.2.cloned.1.call-start = ((), (), s32[]{:S(2)}) async-start(), calls=%async_computation.4 | async-start | bytes 3932160 | tf_op jit(solution)/shard_map/reduce_scatter | solution.py:143
  155.8 8.2 %copy-start.7 = (bf16[1024,512]{0,1:T(8,128)(2,1)S(1)}, bf16[1024,512]{0,1:T(8,128)(2,1)}, u32[]{:S(2)}) copy-start(bf16[1024,512]{0,1:T(8,128)(2,1)} %copy.41) | copy-start | bytes 3145732
  312.6 193.9 %copy-start.10 = (f32[4]{0:T(128)S(1)}, f32[4]{0:T(128)}, u32[]{:S(2)}) copy-start(f32[4]{0:T(128)} %param.27) | copy-start | bytes 52
  312.6 196.2 %copy-start.11 = (f32[128]{0:T(128)S(1)}, f32[128]{0:T(128)}, u32[]{:S(2)}) copy-start(f32[128]{0:T(128)} %param.29) | copy-start | bytes 1540
  330.6 5.8 %copy-start.1 = (bf16[1024,512]{0,1:T(8,128)(2,1)S(1)}, bf16[1024,512]{0,1:T(8,128)(2,1)}, u32[]{:S(2)}) copy-start(bf16[1024,512]{0,1:T(8,128)(2,1)} %get-tuple-element.220) | copy-start | bytes 3145732 | tf_op jit(solution)/shard_map/while
  330.6 5.8 %copy-start.5 = (f32[768,4,128]{0,2,1:T(8,128)S(1)}, f32[768,4,128]{0,2,1:T(8,128)}, u32[]{:S(2)}) copy-start(f32[768,4,128]{0,2,1:T(8,128)} %get-tuple-element.238) | copy-start | bytes 4718596 | tf_op jit(solution)/shard_map/while
  339.7 5.2 copy-start.6
  363.0 5.8 %copy-start.1 = (bf16[1024,512]{0,1:T(8,128)(2,1)S(1)}, bf16[1024,512]{0,1:T(8,128)(2,1)}, u32[]{:S(2)}) copy-start(bf16[1024,512]{0,1:T(8,128)(2,1)} %get-tuple-element.220) | copy-start | bytes 3145732 | tf_op jit(solution)/shard_map/while
  363.0 5.8 %copy-start.5 = (f32[768,4,128]{0,2,1:T(8,128)S(1)}, f32[768,4,128]{0,2,1:T(8,128)}, u32[]{:S(2)}) copy-start(f32[768,4,128]{0,2,1:T(8,128)} %get-tuple-element.238) | copy-start | bytes 4718596 | tf_op jit(solution)/shard_map/while
  372.0 5.2 copy-start.6
  395.3 5.8 %copy-start.1 = (bf16[1024,512]{0,1:T(8,128)(2,1)S(1)}, bf16[1024,512]{0,1:T(8,128)(2,1)}, u32[]{:S(2)}) copy-start(bf16[1024,512]{0,1:T(8,128)(2,1)} %get-tuple-element.220) | copy-start | bytes 3145732 | tf_op jit(solution)/shard_map/while
  395.3 5.8 %copy-start.5 = (f32[768,4,128]{0,2,1:T(8,128)S(1)}, f32[768,4,128]{0,2,1:T(8,128)}, u32[]{:S(2)}) copy-start(f32[768,4,128]{0,2,1:T(8,128)} %get-tuple-element.238) | copy-start | bytes 4718596 | tf_op jit(solution)/shard_map/while
  427.6 5.8 %copy-start.1 = (bf16[1024,512]{0,1:T(8,128)(2,1)S(1)}, bf16[1024,512]{0,1:T(8,128)(2,1)}, u32[]{:S(2)}) copy-start(bf16[1024,512]{0,1:T(8,128)(2,1)} %get-tuple-element.220) | copy-start | bytes 3145732 | tf_op jit(solution)/shard_map/while
  427.6 5.8 %copy-start.5 = (f32[768,4,128]{0,2,1:T(8,128)S(1)}, f32[768,4,128]{0,2,1:T(8,128)}, u32[]{:S(2)}) copy-start(f32[768,4,128]{0,2,1:T(8,128)} %get-tuple-element.238) | copy-start | bytes 4718596 | tf_op jit(solution)/shard_map/while
  459.9 5.8 %copy-start.1 = (bf16[1024,512]{0,1:T(8,128)(2,1)S(1)}, bf16[1024,512]{0,1:T(8,128)(2,1)}, u32[]{:S(2)}) copy-start(bf16[1024,512]{0,1:T(8,128)(2,1)} %get-tuple-element.220) | copy-start | bytes 3145732 | tf_op jit(solution)/shard_map/while
  459.9 5.8 %copy-start.5 = (f32[768,4,128]{0,2,1:T(8,128)S(1)}, f32[768,4,128]{0,2,1:T(8,128)}, u32[]{:S(2)}) copy-start(f32[768,4,128]{0,2,1:T(8,128)} %get-tuple-element.238) | copy-start | bytes 4718596 | tf_op jit(solution)/shard_map/while
  492.2 5.8 %copy-start.1 = (bf16[1024,512]{0,1:T(8,128)(2,1)S(1)}, bf16[1024,512]{0,1:T(8,128)(2,1)}, u32[]{:S(2)}) copy-start(bf16[1024,512]{0,1:T(8,128)(2,1)} %get-tuple-element.220) | copy-start | bytes 3145732 | tf_op jit(solution)/shard_map/while
  492.2 5.8 %copy-start.5 = (f32[768,4,128]{0,2,1:T(8,128)S(1)}, f32[768,4,128]{0,2,1:T(8,128)}, u32[]{:S(2)}) copy-start(f32[768,4,128]{0,2,1:T(8,128)} %get-tuple-element.238) | copy-start | bytes 4718596 | tf_op jit(solution)/shard_map/while
  509.1 39.8 %copy-start.2 = (bf16[192,2048]{1,0:T(8,128)(2,1)S(1)}, bf16[192,2048]{1,0:T(8,128)(2,1)}, u32[]{:S(2)}) copy-start(bf16[192,2048]{1,0:T(8,128)(2,1)} %param.16) | copy-start | bytes 2359300
  509.1 39.8 %copy-start.8 = (f32[1,1,2048]{2,0,1:T(1,128)S(1)}, f32[1,1,2048]{2,0,1:T(1,128)}, u32[]{:S(2)}) copy-start(f32[1,1,2048]{2,0,1:T(1,128)} %get-tuple-element.125) | copy-start | bytes 24580
  (7 other events, 28.3 us)
Sparse Core Ops, SparseCore 0:
  58.6 25.7 all-gather.3
  86.6 49.0 all-gather.5
  137.9 174.6 all-gather.7
  512.8 36.0 reduce-scatter.1
where the time goes:
time: 559 us; the launch traced here: 558 us
  waiting for transfers between devices  232 us (42%)
  matrix products  145 us (26%)
  local copies, waits for them, and re-layouts  72.2 us (13%)
  other arithmetic  49.9 us (9%)
  blocking collectives  44 us (8%)
  between operations  13.3 us (2%)
    all_gather x1, waiting for transfers between devices, per_device(): portion = lax.all_gather(latent_kv, 'sp', axis=0, tiled=True)  136 us
    dot_general x14, matrix products, absorb(): jnp.einsum('hqk,khd->qhd', raised.astype(jnp.bfloat16), value_rows, prefe...  66.5 us
    dot_general x14, matrix products, absorb(): jnp.einsum('qhd,khd->hqk', queries[:, :, which_map], key_rows[:, :, which...  59 us
    dynamic_slice x12, local copies, waits for them, and re-layouts, absorb_rows(): running, unused = lax.scan(advance, running, (stacked, flag_blocks))  42.2 us
    all_gather x1, waiting for transfers between devices, per_device(): every_context = lax.all_gather(context_kv, 'sp', axis=0, tiled=True)  39.3 us
    reduce_sum x7, other arithmetic, absorb(): weight = weight * faded + jnp.sum(raised, axis=2)  39 us
    psum x1, blocking collectives, per_device(): summed = lax.psum(partials, 'sp')  38.8 us
    reduce_scatter x1, waiting for transfers between devices, per_device(): lax.psum_scatter(jnp.dot(flattened, w_out, preferred_element_type=jnp.flo...  36.2 us
  transfers between devices with their start and end apart: 4, of which 4 were waited for; matrix products, arithmetic and copies ran while one was open for 10% of the time, Pallas kernels for 0%

commit v1 on v0

--- a/solution.py
+++ b/solution.py
@@ -98,7 +98,10 @@
         ],
         axis=1,
     )
-    summed = lax.psum(partials, "sp")
+    size, summed = (lax.axis_size("sp"), partials)
+    for far in [1 << k for k in range(size.bit_length() - 1)]:
+        pairs = [(i, i ^ far) for i in range(size)]
+        summed = summed + lax.ppermute(summed, "sp", pairs)
     modulation = lax.all_gather(summed, "tp", axis=2, tiled=True)
     own_rows = modulated(latent, norm_gain, modulation[0, 0], modulation[0, 1])
     context_rows = modulated(context, norm_gain, modulation[1, 0], modulation[1, 1])

time: 559 us -> 537 us (0.961)
  blocking collectives: 44 us -> 5.22 us
  starting transfers between devices: 0.31 us -> 8.61 us
  waiting for transfers between devices: 232 us -> 240 us
    psum x1 -> x0, blocking collectives: 38.8 us -> none  [per_device(): summed = lax.psum(partials, 'sp')]
    ppermute x0 -> x3, starting transfers between devices: none -> 8.3 us  [per_device(): summed = summed + lax.ppermute(summed, 'sp', pairs)]
  transfers between devices with their start and end apart: 4 -> 7, of which waited for: 4 -> 7; matrix products, arithmetic and copies ran while one was open for 10% -> 11% of each run, Pallas kernels for 0% -> 0%
where the time goes in v1:
time: 537 us; the launch traced here: 535 us
  waiting for transfers between devices  240 us (45%)
  matrix products  145 us (27%)
  local copies, waits for them, and re-layouts  72.1 us (13%)
  other arithmetic  49.9 us (9%)
  between operations  13.3 us (2%)
  starting transfers between devices  8.61 us (2%)
    all_gather x1, waiting for transfers between devices, per_device(): portion = lax.all_gather(latent_kv, 'sp', axis=0, tiled=True)  136 us
    dot_general x14, matrix products, absorb(): jnp.einsum('hqk,khd->qhd', raised.astype(jnp.bfloat16), value_rows, prefe...  66.5 us
    dot_general x14, matrix products, absorb(): jnp.einsum('qhd,khd->hqk', queries[:, :, which_map], key_rows[:, :, which...  59 us
    dynamic_slice x12, local copies, waits for them, and re-layouts, absorb_rows(): running, unused = lax.scan(advance, running, (stacked, flag_blocks))  42 us
    all_gather x1, waiting for transfers between devices, per_device(): every_context = lax.all_gather(context_kv, 'sp', axis=0, tiled=True)  39.3 us
    reduce_sum x7, other arithmetic, absorb(): weight = weight * faded + jnp.sum(raised, axis=2)  39 us
    reduce_scatter x1, waiting for transfers between devices, per_device(): lax.psum_scatter(jnp.dot(flattened, w_out, preferred_element_type=jnp.flo...  36.2 us
    all_gather x1, waiting for transfers between devices, per_device(): lax.all_gather(own_rows, 'tp', axis=0, tiled=True)  25 us
  transfers between devices with their start and end apart: 7, of which 7 were waited for; matrix products, arithmetic and copies ran while one was open for 11% of the time, Pallas kernels for 0%

profile of v1, /device:TPU:0, one launch (start us, length us, event | category | flops | bytes accessed | tf_op | source)
XLA Modules:
  0.0 535.1 jit_solution(4041627896141865876)
XLA Ops:
  23.4 5.2 all_gather.12
  36.9 25.0 %all-gather.4.cloned.1.call-done = bf16[768,2048]{1,0:T(8,128)(2,1)} async-done(((bf16[192,2048]{1,0:T(8,128)(2,1)}), bf16[768,2048]{1,0:T(8,128)(2,1)}) %all-gather.4.cloned.1.call-update) | async-done | bytes 3145744 | tf_op jit(solution)/shard_map/all_gather | solution.py:111
  61.9 8.8 %fusion.44 = bf16[768,1536]{1,0:T(8,128)(2,1)S(1)} fusion(bf16[768,2048]{1,0:T(8,128)(2,1)} %all-gather.4.cloned.1.call-done, bf16[2048,512]{1,0:T(8,128)(2,1)} %param.25, bf16[2048,512]{1,0:T(8,128)(2,1)} %param.24, bf16[2048,512]{1,0:T(8,128)(2,1)} %param.23), kind=kOutput, calls=%fused_computation.56 | convolution fusion | flops 4851892224 | bytes 11796480 | tf_op jit(solution)/shard_map/dot_general | solution.py:110
  73.9 39.3 %all-gather.6.cloned.1.call-done = bf16[1024,1024]{1,0:T(8,128)(2,1)} async-done(((bf16[128,1024]{1,0:T(8,128)(2,1)}), bf16[1024,1024]{1,0:T(8,128)(2,1)}) %all-gather.6.cloned.1.call-update) | async-done | bytes 2097168 | tf_op jit(solution)/shard_map/all_gather | solution.py:128
  127.1 6.2 %fusion.25 = (f32[4,768]{1,0:T(4,128)S(1)}, f32[4,768]{1,0:T(4,128)S(1)}, f32[4,768,1024]{2,1,0:T(8,128)}) fusion(f32[4]{0:T(128)S(1)} %copy-done.9, f32[4,768,1024]{2,1,0:T(8,128)S(1)} %fusion.67, bf16[1024,4,2,64]{0,3,2,1:T(8,128)(2,1)S(1)} %bitcast.155, bf16[768,4,2,64]{0,3,2,1:T(8,128)(2,1)S(1)} %bitcast.153), kind=kOutput, calls=%fused_computation.39 | convolution fusion | flops 421521408 | bytes 26108416 | tf_op jit(solution)/shard_map/qhd,khd->hqk/dot_general | solution.py:35
  133.3 8.2 %fusion.29 = (f32[4,768]{1,0:T(4,128)S(1)}, f32[4,768]{1,0:T(4,128)S(1)}) fusion(f32[4,768,1024]{2,1,0:T(8,128)} %get-tuple-element.134, f32[4,768]{1,0:T(4,128)S(1)} %broadcast_maximum_fusion, f32[4]{0:T(128)S(1)} %copy-done.9, f32[4,768]{1,0:T(4,128)S(1)} %broadcast_maximum_fusion.1, f32[4,768,1024]{2,1,0:T(8,128)S(1)} %fusion.67), kind=kLoop, calls=%fused_computation.43 | loop fusion | flops 25159680 | bytes 25214992 | tf_op jit(solution)/shard_map/reduce_sum | solution.py:47
  141.5 8.6 %bitcast_add_fusion.2 = f32[768,4,128]{0,2,1:T(8,128)} fusion(bf16[1024,4,128]{0,2,1:T(8,128)(2,1)S(1)} %bitcast.156, f32[4,768,1024]{2,1,0:T(8,128)} %get-tuple-element.134, f32[4,768]{1,0:T(4,128)S(1)} %broadcast_maximum_fusion, f32[4]{0:T(128)S(1)} %copy-done.9, f32[768,4]{0,1:T(4,128)S(1)} %get-tuple-element.136), kind=kOutput, calls=%fused_computation.67 | convolution fusion | flops 818282496 | bytes 15228944 | tf_op jit(solution)/shard_map/hqk,khd->qhd/dot_general | solution.py:48
  154.2 135.8 %all-gather.8.cloned.1.call-done = bf16[6144,1024]{1,0:T(8,128)(2,1)} async-done(((bf16[768,1024]{1,0:T(8,128)(2,1)}), bf16[6144,1024]{1,0:T(8,128)(2,1)}) %all-gather.8.cloned.1.call-update) | async-done | bytes 12582928 | tf_op jit(solution)/shard_map/all_gather | solution.py:136
  290.0 193.8 %while.20 = (s32[]{:T(128)}, f32[4,768]{1,0:T(4,128)S(1)}, f32[4,768]{1,0:T(4,128)S(1)}, f32[768,4,128]{0,2,1:T(8,128)}, f32[4,768]{1,0:T(4,128)S(1)}, /*index=5...) while((s32[]{:T(128)}, f32[4,768]{1,0:T(4,128)S(1)}, ...), condition=%wide.region_11.12_spmd, body=%wide.region_6.11_spmd.sunk | while | flops 2486716416 | bytes 128058136 | solution.py:69
  302.6 5.5 %bitcast_reduce_fusion.3 = (f32[4,768]{1,0:T(4,128)S(1)}, f32[4,768]{1,0:T(4,128)S(1)}, f32[4,1024,768]{2,1,0:T(8,128)S(1)}) fusion(f32[4]{0:T(128)S(1)} %broadcast_multiply_fusion.2, f32[4,1024,768]{2,1,0:T(8,128)S(1)} %fusion.117, bf16[768,4,2,64]{0,3,1,2:T(8,128)(2,1)} %get-tuple-element.254, bf16[1024,4,2,64]{0,3,2,1:T(8,128)(2,1)S(1)} %bitcast.147), kind=kOutput, calls=%fused_computation.1.clone.1 | convolution fusion | flops 421521408 | bytes 26108416 | tf_op jit(solution)/shard_map/while/body/eval_jaxpr/qhd,khd->hqk/dot_general | solution.py:35
  308.1 5.8 %bitcast_add_fusion.7 = f32[768,4,128]{0,2,1:T(8,128)} fusion(f32[768,4,128]{0,2,1:T(8,128)} %get-tuple-element.241, bf16[1024,4,128]{0,2,1:T(8,128)(2,1)} %bitcast.148, f32[4,1024,768]{2,1,0:T(8,128)S(1)} %get-tuple-element.214, f32[4,768]{1,0:T(4,128)S(1)} %get-tuple-element.250, f32[4]{0:T(128)S(1)} %broadcast_multiply_fusion.2, ...), kind=kOutput, calls=%fused_computation.14.clone.1 | convolution fusion | flops 818675712 | bytes 16801808 | tf_op jit(solution)/shard_map/while/body/eval_jaxpr/hqk,khd->qhd/dot_general | solution.py:48
  334.9 5.5 %bitcast_reduce_fusion.3 = (f32[4,768]{1,0:T(4,128)S(1)}, f32[4,768]{1,0:T(4,128)S(1)}, f32[4,1024,768]{2,1,0:T(8,128)S(1)}) fusion(f32[4]{0:T(128)S(1)} %broadcast_multiply_fusion.2, f32[4,1024,768]{2,1,0:T(8,128)S(1)} %fusion.117, bf16[768,4,2,64]{0,3,1,2:T(8,128)(2,1)} %get-tuple-element.254, bf16[1024,4,2,64]{0,3,2,1:T(8,128)(2,1)S(1)} %bitcast.147), kind=kOutput, calls=%fused_computation.1.clone.1 | convolution fusion | flops 421521408 | bytes 26108416 | tf_op jit(solution)/shard_map/while/body/eval_jaxpr/qhd,khd->hqk/dot_general | solution.py:35
  340.4 5.8 %bitcast_add_fusion.7 = f32[768,4,128]{0,2,1:T(8,128)} fusion(f32[768,4,128]{0,2,1:T(8,128)} %get-tuple-element.241, bf16[1024,4,128]{0,2,1:T(8,128)(2,1)} %bitcast.148, f32[4,1024,768]{2,1,0:T(8,128)S(1)} %get-tuple-element.214, f32[4,768]{1,0:T(4,128)S(1)} %get-tuple-element.250, f32[4]{0:T(128)S(1)} %broadcast_multiply_fusion.2, ...), kind=kOutput, calls=%fused_computation.14.clone.1 | convolution fusion | flops 818675712 | bytes 16801808 | tf_op jit(solution)/shard_map/while/body/eval_jaxpr/hqk,khd->qhd/dot_general | solution.py:48
  367.2 5.5 %bitcast_reduce_fusion.3 = (f32[4,768]{1,0:T(4,128)S(1)}, f32[4,768]{1,0:T(4,128)S(1)}, f32[4,1024,768]{2,1,0:T(8,128)S(1)}) fusion(f32[4]{0:T(128)S(1)} %broadcast_multiply_fusion.2, f32[4,1024,768]{2,1,0:T(8,128)S(1)} %fusion.117, bf16[768,4,2,64]{0,3,1,2:T(8,128)(2,1)} %get-tuple-element.254, bf16[1024,4,2,64]{0,3,2,1:T(8,128)(2,1)S(1)} %bitcast.147), kind=kOutput, calls=%fused_computation.1.clone.1 | convolution fusion | flops 421521408 | bytes 26108416 | tf_op jit(solution)/shard_map/while/body/eval_jaxpr/qhd,khd->hqk/dot_general | solution.py:35
  372.7 5.8 %bitcast_add_fusion.7 = f32[768,4,128]{0,2,1:T(8,128)} fusion(f32[768,4,128]{0,2,1:T(8,128)} %get-tuple-element.241, bf16[1024,4,128]{0,2,1:T(8,128)(2,1)} %bitcast.148, f32[4,1024,768]{2,1,0:T(8,128)S(1)} %get-tuple-element.214, f32[4,768]{1,0:T(4,128)S(1)} %get-tuple-element.250, f32[4]{0:T(128)S(1)} %broadcast_multiply_fusion.2, ...), kind=kOutput, calls=%fused_computation.14.clone.1 | convolution fusion | flops 818675712 | bytes 16801808 | tf_op jit(solution)/shard_map/while/body/eval_jaxpr/hqk,khd->qhd/dot_general | solution.py:48
  399.5 5.5 %bitcast_reduce_fusion.3 = (f32[4,768]{1,0:T(4,128)S(1)}, f32[4,768]{1,0:T(4,128)S(1)}, f32[4,1024,768]{2,1,0:T(8,128)S(1)}) fusion(f32[4]{0:T(128)S(1)} %broadcast_multiply_fusion.2, f32[4,1024,768]{2,1,0:T(8,128)S(1)} %fusion.117, bf16[768,4,2,64]{0,3,1,2:T(8,128)(2,1)} %get-tuple-element.254, bf16[1024,4,2,64]{0,3,2,1:T(8,128)(2,1)S(1)} %bitcast.147), kind=kOutput, calls=%fused_computation.1.clone.1 | convolution fusion | flops 421521408 | bytes 26108416 | tf_op jit(solution)/shard_map/while/body/eval_jaxpr/qhd,khd->hqk/dot_general | solution.py:35
  405.0 5.8 %bitcast_add_fusion.7 = f32[768,4,128]{0,2,1:T(8,128)} fusion(f32[768,4,128]{0,2,1:T(8,128)} %get-tuple-element.241, bf16[1024,4,128]{0,2,1:T(8,128)(2,1)} %bitcast.148, f32[4,1024,768]{2,1,0:T(8,128)S(1)} %get-tuple-element.214, f32[4,768]{1,0:T(4,128)S(1)} %get-tuple-element.250, f32[4]{0:T(128)S(1)} %broadcast_multiply_fusion.2, ...), kind=kOutput, calls=%fused_computation.14.clone.1 | convolution fusion | flops 818675712 | bytes 16801808 | tf_op jit(solution)/shard_map/while/body/eval_jaxpr/hqk,khd->qhd/dot_general | solution.py:48
  414.0 5.1 fusion.120
  431.8 5.5 %bitcast_reduce_fusion.3 = (f32[4,768]{1,0:T(4,128)S(1)}, f32[4,768]{1,0:T(4,128)S(1)}, f32[4,1024,768]{2,1,0:T(8,128)S(1)}) fusion(f32[4]{0:T(128)S(1)} %broadcast_multiply_fusion.2, f32[4,1024,768]{2,1,0:T(8,128)S(1)} %fusion.117, bf16[768,4,2,64]{0,3,1,2:T(8,128)(2,1)} %get-tuple-element.254, bf16[1024,4,2,64]{0,3,2,1:T(8,128)(2,1)S(1)} %bitcast.147), kind=kOutput, calls=%fused_computation.1.clone.1 | convolution fusion | flops 421521408 | bytes 26108416 | tf_op jit(solution)/shard_map/while/body/eval_jaxpr/qhd,khd->hqk/dot_general | solution.py:35
  437.3 5.8 %bitcast_add_fusion.7 = f32[768,4,128]{0,2,1:T(8,128)} fusion(f32[768,4,128]{0,2,1:T(8,128)} %get-tuple-element.241, bf16[1024,4,128]{0,2,1:T(8,128)(2,1)} %bitcast.148, f32[4,1024,768]{2,1,0:T(8,128)S(1)} %get-tuple-element.214, f32[4,768]{1,0:T(4,128)S(1)} %get-tuple-element.250, f32[4]{0:T(128)S(1)} %broadcast_multiply_fusion.2, ...), kind=kOutput, calls=%fused_computation.14.clone.1 | convolution fusion | flops 818675712 | bytes 16801808 | tf_op jit(solution)/shard_map/while/body/eval_jaxpr/hqk,khd->qhd/dot_general | solution.py:48
  446.3 5.1 fusion.120
  464.1 5.5 %bitcast_reduce_fusion.3 = (f32[4,768]{1,0:T(4,128)S(1)}, f32[4,768]{1,0:T(4,128)S(1)}, f32[4,1024,768]{2,1,0:T(8,128)S(1)}) fusion(f32[4]{0:T(128)S(1)} %broadcast_multiply_fusion.2, f32[4,1024,768]{2,1,0:T(8,128)S(1)} %fusion.117, bf16[768,4,2,64]{0,3,1,2:T(8,128)(2,1)} %get-tuple-element.254, bf16[1024,4,2,64]{0,3,2,1:T(8,128)(2,1)S(1)} %bitcast.147), kind=kOutput, calls=%fused_computation.1.clone.1 | convolution fusion | flops 421521408 | bytes 26108416 | tf_op jit(solution)/shard_map/while/body/eval_jaxpr/qhd,khd->hqk/dot_general | solution.py:35
  469.6 5.8 %bitcast_add_fusion.7 = f32[768,4,128]{0,2,1:T(8,128)} fusion(f32[768,4,128]{0,2,1:T(8,128)} %get-tuple-element.241, bf16[1024,4,128]{0,2,1:T(8,128)(2,1)} %bitcast.148, f32[4,1024,768]{2,1,0:T(8,128)S(1)} %get-tuple-element.214, f32[4,768]{1,0:T(4,128)S(1)} %get-tuple-element.250, f32[4]{0:T(128)S(1)} %broadcast_multiply_fusion.2, ...), kind=kOutput, calls=%fused_computation.14.clone.1 | convolution fusion | flops 818675712 | bytes 16801808 | tf_op jit(solution)/shard_map/while/body/eval_jaxpr/hqk,khd->qhd/dot_general | solution.py:48
  490.0 36.2 %reduce-scatter.2.cloned.1.call-done = bf16[192,2048]{1,0:T(8,128)(2,1)} async-done(((bf16[768,2048]{1,0:T(8,128)(2,1)}), bf16[192,2048]{1,0:T(8,128)(2,1)}) %reduce-scatter.2.cloned.1.call-update) | async-done | bytes 786448 | tf_op jit(solution)/shard_map/reduce_scatter | solution.py:146
  (169 shorter events, 170.1 us)
Async XLA Ops:
  6.5 480.0 %copy-start = (bf16[512,2048]{1,0:T(8,128)(2,1)S(1)}, bf16[512,2048]{1,0:T(8,128)(2,1)}, u32[]{:S(2)}) copy-start(bf16[512,2048]{1,0:T(8,128)(2,1)} %param.26) | copy-start | bytes 6291460
  6.5 55.4 %all-gather.4.cloned.1.call-start = ((), (), s32[]{:S(2)}) async-start(), calls=%async_computation.1 | async-start | bytes 3932160 | tf_op jit(solution)/shard_map/all_gather | solution.py:111
  10.0 4.7 collective-permute-start
  14.8 3.8 collective-permute-start.1
  18.6 4.8 collective-permute-start.2
  31.7 81.5 %all-gather.6.cloned.1.call-start = ((), (), s32[]{:S(2)}) async-start(), calls=%async_computation.2 | async-start | bytes 2359296 | tf_op jit(solution)/shard_map/all_gather | solution.py:128
  36.9 253.2 %all-gather.8.cloned.1.call-start = ((), (), s32[]{:S(2)}) async-start(), calls=%async_computation.3 | async-start | bytes 14155776 | tf_op jit(solution)/shard_map/all_gather | solution.py:136
  73.6 452.6 %reduce-scatter.2.cloned.1.call-start = ((), (), s32[]{:S(2)}) async-start(), calls=%async_computation.4 | async-start | bytes 3932160 | tf_op jit(solution)/shard_map/reduce_scatter | solution.py:146
  133.3 8.2 %copy-start.7 = (bf16[1024,512]{0,1:T(8,128)(2,1)S(1)}, bf16[1024,512]{0,1:T(8,128)(2,1)}, u32[]{:S(2)}) copy-start(bf16[1024,512]{0,1:T(8,128)(2,1)} %copy.41) | copy-start | bytes 3145732
  290.0 193.8 %copy-start.10 = (f32[4]{0:T(128)S(1)}, f32[4]{0:T(128)}, u32[]{:S(2)}) copy-start(f32[4]{0:T(128)} %param.27) | copy-start | bytes 52
  290.0 196.1 %copy-start.11 = (f32[128]{0:T(128)S(1)}, f32[128]{0:T(128)}, u32[]{:S(2)}) copy-start(f32[128]{0:T(128)} %param.29) | copy-start | bytes 1540
  308.1 5.8 %copy-start.1 = (bf16[1024,512]{0,1:T(8,128)(2,1)S(1)}, bf16[1024,512]{0,1:T(8,128)(2,1)}, u32[]{:S(2)}) copy-start(bf16[1024,512]{0,1:T(8,128)(2,1)} %get-tuple-element.220) | copy-start | bytes 3145732 | tf_op jit(solution)/shard_map/while
  340.4 5.8 %copy-start.1 = (bf16[1024,512]{0,1:T(8,128)(2,1)S(1)}, bf16[1024,512]{0,1:T(8,128)(2,1)}, u32[]{:S(2)}) copy-start(bf16[1024,512]{0,1:T(8,128)(2,1)} %get-tuple-element.220) | copy-start | bytes 3145732 | tf_op jit(solution)/shard_map/while
  340.4 5.8 %copy-start.5 = (f32[768,4,128]{0,2,1:T(8,128)S(1)}, f32[768,4,128]{0,2,1:T(8,128)}, u32[]{:S(2)}) copy-start(f32[768,4,128]{0,2,1:T(8,128)} %get-tuple-element.238) | copy-start | bytes 4718596 | tf_op jit(solution)/shard_map/while
  372.7 5.8 %copy-start.1 = (bf16[1024,512]{0,1:T(8,128)(2,1)S(1)}, bf16[1024,512]{0,1:T(8,128)(2,1)}, u32[]{:S(2)}) copy-start(bf16[1024,512]{0,1:T(8,128)(2,1)} %get-tuple-element.220) | copy-start | bytes 3145732 | tf_op jit(solution)/shard_map/while
  372.7 5.8 %copy-start.5 = (f32[768,4,128]{0,2,1:T(8,128)S(1)}, f32[768,4,128]{0,2,1:T(8,128)}, u32[]{:S(2)}) copy-start(f32[768,4,128]{0,2,1:T(8,128)} %get-tuple-element.238) | copy-start | bytes 4718596 | tf_op jit(solution)/shard_map/while
  405.0 5.8 %copy-start.1 = (bf16[1024,512]{0,1:T(8,128)(2,1)S(1)}, bf16[1024,512]{0,1:T(8,128)(2,1)}, u32[]{:S(2)}) copy-start(bf16[1024,512]{0,1:T(8,128)(2,1)} %get-tuple-element.220) | copy-start | bytes 3145732 | tf_op jit(solution)/shard_map/while
  405.0 5.8 %copy-start.5 = (f32[768,4,128]{0,2,1:T(8,128)S(1)}, f32[768,4,128]{0,2,1:T(8,128)}, u32[]{:S(2)}) copy-start(f32[768,4,128]{0,2,1:T(8,128)} %get-tuple-element.238) | copy-start | bytes 4718596 | tf_op jit(solution)/shard_map/while
  437.3 5.8 %copy-start.1 = (bf16[1024,512]{0,1:T(8,128)(2,1)S(1)}, bf16[1024,512]{0,1:T(8,128)(2,1)}, u32[]{:S(2)}) copy-start(bf16[1024,512]{0,1:T(8,128)(2,1)} %get-tuple-element.220) | copy-start | bytes 3145732 | tf_op jit(solution)/shard_map/while
  437.3 5.8 %copy-start.5 = (f32[768,4,128]{0,2,1:T(8,128)S(1)}, f32[768,4,128]{0,2,1:T(8,128)}, u32[]{:S(2)}) copy-start(f32[768,4,128]{0,2,1:T(8,128)} %get-tuple-element.238) | copy-start | bytes 4718596 | tf_op jit(solution)/shard_map/while
  469.6 5.8 %copy-start.1 = (bf16[1024,512]{0,1:T(8,128)(2,1)S(1)}, bf16[1024,512]{0,1:T(8,128)(2,1)}, u32[]{:S(2)}) copy-start(bf16[1024,512]{0,1:T(8,128)(2,1)} %get-tuple-element.220) | copy-start | bytes 3145732 | tf_op jit(solution)/shard_map/while
  469.6 5.8 %copy-start.5 = (f32[768,4,128]{0,2,1:T(8,128)S(1)}, f32[768,4,128]{0,2,1:T(8,128)}, u32[]{:S(2)}) copy-start(f32[768,4,128]{0,2,1:T(8,128)} %get-tuple-element.238) | copy-start | bytes 4718596 | tf_op jit(solution)/shard_map/while
  486.5 39.8 %copy-start.2 = (bf16[192,2048]{1,0:T(8,128)(2,1)S(1)}, bf16[192,2048]{1,0:T(8,128)(2,1)}, u32[]{:S(2)}) copy-start(bf16[192,2048]{1,0:T(8,128)(2,1)} %param.16) | copy-start | bytes 2359300
  486.5 39.7 %copy-start.8 = (f32[1,1,2048]{2,0,1:T(1,128)S(1)}, f32[1,1,2048]{2,0,1:T(1,128)}, u32[]{:S(2)}) copy-start(f32[1,1,2048]{2,0,1:T(1,128)} %get-tuple-element.125) | copy-start | bytes 24580
  (10 other events, 44.4 us)
Sparse Core Ops, SparseCore 0:
  31.8 30.0 all-gather.3
  64.0 49.0 all-gather.5
  115.4 174.6 all-gather.7
  490.1 36.0 reduce-scatter.1
